TPU v7x, 512 devices: a whole 4x4x16 slice. The times are simulated.
512 devices in a mesh: sp: 32 (over z, core), tp: 16 (over y, x).
Axes of the slice: x: 4, y: 4, z: 16, core: 2. Of those that a mesh axis runs over, the one named last changes fastest.
Arguments:
- residual: bfloat16 [6144, 2048], P('sp'), may hold values from -6 to 6
- query_in: bfloat16 [6144, 2048], P('sp', 'tp'), may hold values from -6 to 6
- value_in: bfloat16 [6144, 2048], P('sp', 'tp'), may hold values from -6 to 6
- forget_fwd: bfloat16 [6144, 2048], P('sp', 'tp'), may hold values from -4.5 to 4.5
- forget_bwd: bfloat16 [6144, 2048], P('sp', 'tp'), may hold values from -4.5 to 4.5
- jumps: float32 [16, 6144], P('tp', 'sp'), may hold values from -2.8 to 0
- gate_gap: float32 [2, 2048], P(None, 'tp'), may hold values from 0 to 0.1
- out_gate: bfloat16 [6144, 2048], P('sp', 'tp'), may hold values from -6 to 6
- head_gain: float32 [2048], P('tp'), may hold values from 0.1 to 1.9
- out_weight: bfloat16 [2048, 2048], P('tp'), may hold values from -0.25 to 0.25
- norm_gain: float32 [2048], replicated, may hold values from 0.1 to 1.9
- route_ids: int32 [6144, 4], P('sp'), may hold values from 0 to 31, all different within a row; in each aligned block of 192 rows (0 to 191, 192 to 383, ...) at most 36 rows name the same one
- route_weights: float32 [6144, 4], P('sp'), may hold values from 0.05 to 0.5
- w_gate: bfloat16 [32, 2048, 4096], P('sp', None, 'tp'), may hold values from -0.375 to 0.375
- w_up: bfloat16 [32, 2048, 4096], P('sp', None, 'tp'), may hold values from -0.375 to 0.375
- w_down: bfloat16 [32, 4096, 2048], P('sp', None, 'tp'), may hold values from -0.09375 to 0.09375
Outputs:
- mixed: bfloat16 [6144, 2048], P('sp', 'tp')
Inputs may be any that keep to these rules, and one draw needn't show every extreme that they name: `route_ids`: in each aligned block of 192 rows each expert is named by at most 36 rows, and by exactly 36 in some block; each row names 4 different experts.
All inputs are finite; a program needn't handle non-finite values.
Results may differ from a plain program's by a relative error of at most 0.024.
Values may be sent and summed in bfloat16 or wider, within the bound.
A program may use at most 64 MiB of HBM per device.

v0:
```python
import math
import jax
import jax.numpy as jnp
from jax import lax
from jax.sharding import Mesh
from jax.sharding import PartitionSpec as P

EXPERTS = 32
CAP = 36
SP = ("sp_0", "sp_1")
highest_precision = lax.Precision.HIGHEST
eps_norm = 1e-06
limit_value = 7.0
alpha_value = 1.702


def filled_with(x, identity):
    return jax.tree.map(
        lambda a, e: jnp.broadcast_to(jnp.asarray(e, a.dtype), a.shape), x, identity
    )


def all_in_one(x, axis):
    leaves = jax.tree.leaves(x)
    turns = sorted(range(len(leaves)), key=lambda k: -leaves[k].size)
    width = (1, *leaves[turns[0]].shape)[-1]
    lines = [
        jnp.pad(leaves[k].reshape(-1), (0, -leaves[k].size % width)).reshape(-1, width)
        for k in turns
    ]
    both, at, found = (lax.all_gather(jnp.concatenate(lines), axis), 0, {})
    for k, line in zip(turns, lines):
        section = both[:, at : at + len(line)].reshape(len(both), -1)
        found[k] = section[:, : leaves[k].size].reshape(-1, *leaves[k].shape)
        at += len(line)
    numbers = iter(range(len(leaves)))
    return jax.tree.map(lambda _: found[next(numbers)], x)


def entering(x, axes, combine, identity, reverse):
    before = start = filled_with(x, identity)
    running = x
    for axis in reversed(axes):
        length, index = (lax.axis_size(axis), lax.axis_index(axis))
        pieces = all_in_one(
            jax.tree.map(
                lambda part, kind: part.astype(kind),
                running,
                jax.tree.map(lambda a: jnp.bfloat16 if a.dtype == jnp.float32 else a.dtype, x),
            ),
            axis,
        )
        inside, running = (start, start)
        for k in reversed(range(length)) if reverse else range(length):
            passed = k > index if reverse else k < index
            running = combine(
                running, jax.tree.map(lambda part, own: part[k].astype(own.dtype), pieces, x)
            )
            inside = jax.tree.map(lambda new, old: jnp.where(passed, new, old), running, inside)
        before = combine(inside, before)
    return before


def in_blocks(x, dim, length):
    shape = x.shape
    pieces = x.reshape(*shape[:dim], length, shape[dim] // length, *shape[dim + 1 :])
    return jnp.moveaxis(pieces, dim, 0)


def sent_and_summed(x, axis, dim):
    length = lax.axis_size(axis)
    pieces = lax.all_to_all(in_blocks(x, dim, length), axis, 0, 0, tiled=True)
    return jnp.sum(pieces.astype(jnp.float32), axis=0)


def rows_for(lines, length):
    spare = -lines.shape[0] % length
    if not spare:
        return lines
    return jnp.concatenate([lines, jnp.zeros((spare, *lines.shape[1:]), lines.dtype)])


def in_order(pieces, dim):
    pieces = jnp.moveaxis(pieces, 0, dim)
    shape = pieces.shape
    return pieces.reshape(*shape[:dim], shape[dim] * shape[dim + 1], *shape[dim + 2 :])


def sent_to_all(x, axis):
    copies = jnp.broadcast_to(x, (lax.axis_size(axis), *x.shape))
    return lax.all_to_all(copies, axis, split_axis=0, concat_axis=0, tiled=True)


def gather_directly(x, axis, dim):
    return in_order(sent_to_all(x, axis), dim)


def sum_by_parts(x, axes):
    lines = x.reshape(-1, x.shape[-1])
    own = sent_and_summed(rows_for(lines, lax.axis_size(axes)), axes, 0)
    whole = gather_directly(own.astype(jnp.bfloat16), axes, 0)
    return whole[: len(lines)].reshape(x.shape).astype(jnp.float32)


def turned_blocks(pieces, axes, turns):
    inside = pieces.shape[1:]
    filled = pieces.reshape(*(lax.axis_size(a) for a in axes), *inside)
    for k in turns:
        filled = lax.all_to_all(filled, axes[k], k, k, tiled=True)
    return filled.reshape(-1, *inside)


def core_and_chips(x, groups, turns, split_dim, concat_dim):
    length = lax.axis_size(groups[0]) * lax.axis_size(groups[1])
    pieces = in_blocks(x, split_dim, length)
    return in_order(turned_blocks(pieces, groups, turns), concat_dim)


def block_pass(queries, keys_in, values, logs):
    head_rows, head_count, head_width = queries.shape
    block_size = math.gcd(head_rows, 64)
    block_count = head_rows // block_size

    def to_blocks(array):
        return array.reshape(block_count, block_size, head_count, array.shape[-1])

    q_block, k_block, v_block, log_block = (
        to_blocks(queries),
        to_blocks(keys_in),
        to_blocks(values),
        to_blocks(logs),
    )
    decay_sums = jnp.cumsum(log_block, axis=1)
    middle = decay_sums[:, block_size // 2 - 1 : block_size // 2]
    scores = jnp.einsum(
        "nthk,nshk->nhts",
        q_block * jnp.exp(decay_sums - middle),
        k_block * jnp.exp(middle - decay_sums),
        precision=highest_precision,
    )
    lower_mask = jnp.tril(jnp.ones((block_size, block_size), bool))
    within = jnp.einsum(
        "nhts,nshv->nthv", jnp.where(lower_mask, scores, 0.0), v_block, precision=highest_precision
    )
    block_end = decay_sums[:, -1]
    q_start = q_block * jnp.exp(decay_sums)
    k_end = k_block * jnp.exp(block_end[:, None] - decay_sums)

    def advance(current_state, block_items):
        query_segment, key_segment, value_segment, decay_part = block_items
        state_readout = jnp.einsum(
            "qwe,wei->qwi", query_segment, current_state, precision=highest_precision
        )
        current_state = current_state * jnp.exp(decay_part)[:, :, None] + jnp.einsum(
            "foj,fox->ojx", key_segment, value_segment, precision=highest_precision
        )
        return (current_state, state_readout)

    zero_state = jnp.zeros((head_count, head_width, values.shape[-1]), jnp.float32)
    final_state, across = lax.scan(advance, zero_state, (q_start, k_end, v_block, block_end))
    return ((within + across).reshape(head_rows, head_count, -1), final_state)


def combine_states(first_part, second_part):
    return (
        first_part[0] * second_part[0],
        second_part[0][:, :, None] * first_part[1] + second_part[1],
    )


def carried(queries, logs, running_state):
    decayed_state = queries * jnp.exp(jnp.cumsum(logs, axis=0))
    return jnp.einsum("una,nae->une", decayed_state, running_state, precision=highest_precision)


def shards(
    residual,
    query_in,
    value_in,
    forget_fwd,
    forget_bwd,
    jumps,
    gate_gap,
    out_gate,
    head_gain,
    out_weight,
    norm_gain,
    route_ids,
    route_weights,
    w_gate,
    w_up,
    w_down,
):
    head_rows, local_width = query_in.shape
    head_count = jumps.shape[0]
    head_width = local_width // head_count

    def by_head(array):
        return array.astype(jnp.float32).reshape(head_rows, head_count, head_width)

    queries = jax.nn.silu(by_head(query_in))
    values = by_head(value_in)
    jump_rows = jnp.transpose(jumps)[:, :, None]

    def gate_terms(forget_in, gap):
        key_share = gap.reshape(head_count, head_width) * jax.nn.sigmoid(-by_head(forget_in))
        return (key_share, jnp.log1p(-key_share) + jump_rows)

    keys_fwd, logs_fwd = gate_terms(forget_fwd, gate_gap[0])
    keys_bwd, logs_bwd = gate_terms(forget_bwd, gate_gap[1])
    ones_part = jnp.ones((head_count, head_width), jnp.float32)
    zero_part = jnp.zeros((head_count, head_width, head_width), jnp.float32)
    local_fwd, final_fwd = block_pass(queries, keys_fwd, values, logs_fwd)
    summary_fwd = (jnp.exp(jnp.sum(logs_fwd, axis=0)), final_fwd)
    carry_fwd = entering(summary_fwd, SP, combine_states, (ones_part, zero_part), False)[1]
    flip_queries = jnp.flip(queries, 0)
    flip_logs = jnp.flip(logs_bwd, 0)
    local_bwd, final_bwd = block_pass(
        flip_queries, jnp.flip(keys_bwd, 0), jnp.flip(values, 0), flip_logs
    )
    summary_bwd = (jnp.exp(jnp.sum(logs_bwd, axis=0)), final_bwd)
    carry_bwd = entering(summary_bwd, SP, combine_states, (ones_part, zero_part), True)[1]
    forward_out = local_fwd + carried(queries, logs_fwd, carry_fwd)
    backward_out = jnp.flip(local_bwd + carried(flip_queries, flip_logs, carry_bwd), 0)
    mixed_heads = forward_out + backward_out
    mean_square = jnp.mean(mixed_heads * mixed_heads, axis=-1, keepdims=True)
    normed = (mixed_heads * lax.rsqrt(mean_square + eps_norm)).reshape(head_rows, local_width)
    gated = (normed * head_gain * jax.nn.silu(out_gate.astype(jnp.float32))).astype(jnp.bfloat16)
    head_terms = jnp.dot(gated, out_weight, preferred_element_type=jnp.float32)
    summed = sum_by_parts(head_terms.astype(jnp.bfloat16), "tp")
    stream = (residual.astype(jnp.float32) + summed).astype(jnp.bfloat16)
    stream_f = stream.astype(jnp.float32)
    row_scale = lax.rsqrt(jnp.mean(stream_f * stream_f, axis=-1, keepdims=True) + eps_norm)
    normed_rows = (stream_f * row_scale * norm_gain).astype(jnp.bfloat16)
    top_count = route_ids.shape[1]
    flat_ids = route_ids.reshape(-1)
    one_hot = (flat_ids[:, None] == jnp.arange(EXPERTS, dtype=jnp.int32)[None, :]).astype(jnp.int32)
    slot_rank = jnp.sum((jnp.cumsum(one_hot, axis=0) - 1) * one_hot, axis=1)
    slot_index = flat_ids * CAP + slot_rank
    owner_rows = jnp.arange(head_rows * top_count, dtype=jnp.int32) // top_count
    slot_rows = jnp.full((EXPERTS * CAP,), head_rows, jnp.int32).at[slot_index].set(owner_rows)
    padded_rows = jnp.concatenate(
        [normed_rows, jnp.zeros((1, normed_rows.shape[1]), jnp.bfloat16)], axis=0
    )
    tp_index = lax.axis_index("tp")
    part_width = w_down.shape[2]
    column_rows = lax.dynamic_slice_in_dim(padded_rows, tp_index * part_width, part_width, 1)
    buffer = column_rows[slot_rows].reshape(EXPERTS, CAP, part_width)
    arrived = lax.all_to_all(buffer, SP, split_axis=0, concat_axis=1, tiled=True)
    piece = lax.all_gather(arrived, "tp", axis=2, tiled=True)
    gate_sum = jnp.einsum("esd,edf->esf", piece, w_gate, preferred_element_type=jnp.float32)
    up_sum = jnp.einsum("esd,edf->esf", piece, w_up, preferred_element_type=jnp.float32)
    gate_sum = jnp.minimum(gate_sum, limit_value)
    up_sum = jnp.clip(up_sum, -limit_value, limit_value)
    active = (gate_sum * jax.nn.sigmoid(alpha_value * gate_sum) * (up_sum + 1.0)).astype(
        jnp.bfloat16
    )
    produced = jnp.einsum(
        "esf,efd->esd",
        lax.all_gather(active, "tp", axis=2, tiled=True),
        w_down,
        preferred_element_type=jnp.float32,
    ).astype(jnp.bfloat16)
    returned = core_and_chips(produced, ("sp_0", "sp_1"), (1, 0), 1, 0)
    picked = returned.reshape(EXPERTS * CAP, part_width)[slot_index].astype(jnp.float32)
    picked = picked.reshape(head_rows, top_count, part_width)
    moe_out = jnp.sum(picked * route_weights[:, :, None], axis=1)
    own_columns = lax.dynamic_slice_in_dim(stream_f, tp_index * part_width, part_width, 1)
    return (own_columns + moe_out).astype(jnp.bfloat16)


def solution(mesh):
    finer = Mesh(mesh.devices.reshape(16, 2, mesh.shape["tp"]), ("sp_0", "sp_1", "tp"))
    return jax.shard_map(
        shards,
        mesh=finer,
        in_specs=(
            P(SP, None),
            P(SP, "tp"),
            P(SP, "tp"),
            P(SP, "tp"),
            P(SP, "tp"),
            P("tp", SP),
            P(None, "tp"),
            P(SP, "tp"),
            P("tp"),
            P("tp", None),
            P(),
            P(SP, None),
            P(SP, None),
            P(SP, None, "tp"),
            P(SP, None, "tp"),
            P(SP, None, "tp"),
        ),
        out_specs=P(SP, "tp"),
        check_vma=False,
    )
```

profile of v0, /device:TPU:2, one launch (start us, length us, event | category | flops | bytes accessed | tf_op | source)
XLA Modules:
  0.0 397.6 jit_solution(2136767596949991621)
XLA Ops:
  6.5 0.8 slice_bitcast_fusion.35
  7.3 1.0 fusion.388
  8.4 0.8 convert_multiply_fusion.2
  9.2 0.8 convert_element_type.809
  10.1 0.5 copy_bitcast_fusion.2
  10.6 0.2 exponential_multiply_fusion.2
  10.9 1.7 while.26
  11.1 0.3 fusion.427
  11.7 0.3 fusion.427
  12.3 0.3 fusion.427
  12.6 1.9 all-gather.5
  14.5 0.6 broadcast_select_fusion.3
  15.2 38.4 %all-gather.6 = bf16[16,129,128]{2,1,0:T(8,128)(2,1)S(1)} all-gather(bf16[1,129,128]{2,1,0:T(8,128)(2,1)S(1)} %maximum_bitcast_fusion.1), channel_id=3, replica_groups=mesh['sp_0'=16,'sp_1'=2,'tp'=16] {'sp_0'}, dimensions={0}, use_global_device_ids=true | all-gather | bytes 561408 | tf_op jit(solution)/shard_map/all_gather | solution.py:31
  53.6 0.6 fusion.381
  54.2 0.5 fusion.366
  54.9 0.2 reverse.15
  55.2 0.2 reverse.13
  55.5 0.2 reverse.14
  55.7 0.6 copy_bitcast_fusion
  56.3 0.2 exponential_multiply_fusion
  56.6 1.7 while.27
  56.9 0.3 fusion.434
  57.4 0.3 fusion.434
  58.0 0.3 fusion.434
  58.4 1.9 all-gather.7
  60.2 0.6 broadcast_select_fusion.1
  61.0 29.2 %all-gather.8 = bf16[16,129,128]{2,1,0:T(8,128)(2,1)S(1)} all-gather(bf16[1,129,128]{2,1,0:T(8,128)(2,1)S(1)} %maximum_bitcast_fusion.3), channel_id=5, replica_groups=mesh['sp_0'=16,'sp_1'=2,'tp'=16] {'sp_0'}, dimensions={0}, use_global_device_ids=true | all-gather | bytes 561408 | tf_op jit(solution)/shard_map/all_gather | solution.py:31
  90.2 0.6 fusion.364
  90.8 0.5 fusion.349
  91.8 0.3 convolution_select_fusion
  92.2 1.1 fusion.41
  93.5 1.5 fusion.39
  95.0 0.2 rev.14
  95.3 0.3 convolution_select_fusion.1
  96.0 1.6 multiply_reduce_fusion.1
  97.7 0.4 convolution_convert_fusion
  98.1 1.2 reshape.1657
  99.3 7.5 %all-to-all-start = ((bf16[16,12,2048]{2,1,0:T(8,128)(2,1)}), bf16[16,12,2048]{2,1,0:T(8,128)(2,1)S(1)}, u32[]{:S(2)}, u32[]{:S(2)}) async-start(bf16[16,12,2048]{2,1,0:T(8,128)(2,1)} %reshape.1657), calls=%async_computation | async-start | bytes 2097152 | tf_op jit(solution)/shard_map/all_to_all | solution.py:72
  107.0 1.7 reduce-window.26
  108.7 9.9 %all-to-all-done = bf16[16,12,2048]{2,1,0:T(8,128)(2,1)S(1)} async-done(((bf16[16,12,2048]{2,1,0:T(8,128)(2,1)}), bf16[16,12,2048]{2,1,0:T(8,128)(2,1)S(1)}, u32[]{:S(2)}, u32[]{:S(2)}) %all-to-all-start) | async-done | bytes 786464 | tf_op jit(solution)/shard_map/all_to_all | solution.py:72
  118.8 1.1 broadcast_in_dim.35
  120.0 5.0 %all-to-all-start.1 = ((bf16[16,12,2048]{2,1,0:T(8,128)(2,1)}), bf16[16,12,2048]{2,1,0:T(8,128)(2,1)S(1)}, u32[]{:S(2)}, u32[]{:S(2)}) async-start(bf16[16,12,2048]{2,1,0:T(8,128)(2,1)} %broadcast_in_dim.35), calls=%async_computation.1 | async-start | bytes 2097152 | tf_op jit(solution)/shard_map/all_to_all | solution.py:91
  125.0 0.3 slice_reduce_fusion
  125.7 3.4 scatter_custom_fusion
  129.2 7.8 %all-to-all-done.1 = bf16[16,12,2048]{2,1,0:T(8,128)(2,1)S(1)} async-done(((bf16[16,12,2048]{2,1,0:T(8,128)(2,1)}), bf16[16,12,2048]{2,1,0:T(8,128)(2,1)S(1)}, u32[]{:S(2)}, u32[]{:S(2)}) %all-to-all-start.1) | async-done | bytes 786464 | tf_op jit(solution)/shard_map/all_to_all | solution.py:91
  136.9 1.3 reshape.1699
  138.3 1.7 multiply_reduce_fusion
  140.0 0.2 multiply_convert_fusion
  140.2 2.9 gather_fusion
  143.2 33.2 %all_to_all.32 = bf16[32,36,128]{2,1,0:T(8,128)(2,1)S(1)} all-to-all(bf16[32,36,128]{2,1,0:T(8,128)(2,1)S(1)} %reshape.1659), channel_id=1, replica_groups=mesh['sp_0'=16,'sp_1'=2,'tp'=16] {'sp_0','sp_1'}, dimensions={0} | all-to-all | bytes 589824 | tf_op jit(solution)/shard_map/all_to_all | solution.py:249
  176.5 0.8 all_to_all.24
  177.3 0.2 all-gather.14.cloned.1.call-start
  177.5 62.6 %all-gather.12.cloned.1.call-done = bf16[1,1152,2048]{2,1,0:T(8,128)(2,1)} async-done(((bf16[1,1152,128]{2,1,0:T(8,128)(2,1)}), bf16[1,1152,2048]{2,1,0:T(8,128)(2,1)}) %all-gather.12.cloned.1.call-update) | async-done | bytes 4718608 | tf_op jit(solution)/shard_map/all_gather | solution.py:250
  240.1 3.9 fusion.25
  244.1 2.4 fusion.34
  246.6 97.4 %all-gather.14.cloned.1.call-done = bf16[1152,4096]{1,0:T(8,128)(2,1)} async-done(((bf16[1152,256]{1,0:T(8,128)(2,1)}), bf16[1152,4096]{1,0:T(8,128)(2,1)}) %all-gather.14.cloned.1.call-update) | async-done | bytes 9437200 | tf_op jit(solution)/shard_map/all_gather | solution.py:260
  344.0 6.5 %convolution_convert_fusion.1 = bf16[1152,128]{1,0:T(8,128)(2,1)S(1)} fusion(bf16[1152,4096]{1,0:T(8,128)(2,1)} %all-gather.14.cloned.1.call-done, bf16[1,4096,128]{2,1,0:T(8,128)(2,1)} %param.35), kind=kOutput, calls=%fused_computation.43 | convolution fusion | flops 1208107008 | bytes 10780672 | tf_op jit(solution)/shard_map/esf,efd->esd/dot_general | solution.py:258
  350.7 4.0 all_to_all.33
  354.6 1.0 copy.64
  355.6 12.3 %all-to-all-start.4 = ((bf16[16,2,1,36,128]{4,1,3,2,0:T(2,128)(2,1)}), bf16[16,2,1,36,128]{4,1,3,2,0:T(2,128)(2,1)S(1)}, u32[]{:S(2)}, u32[]{:S(2)}) async-start(bf16[16,2,1,36,128]{4,1,3,2,0:T(2,128)(2,1)} %copy.64), calls=%async_computation.4 | async-start | bytes 589824 | tf_op jit(solution)/shard_map/all_to_all | solution.py:109
  368.1 19.8 %all-to-all-done.4 = bf16[16,2,1,36,128]{4,1,3,2,0:T(2,128)(2,1)S(1)} async-done(((bf16[16,2,1,36,128]{4,1,3,2,0:T(2,128)(2,1)}), bf16[16,2,1,36,128]{4,1,3,2,0:T(2,128)(2,1)S(1)}, u32[]{:S(2)}, u32[]{:S(2)}) %all-to-all-start.4) | async-done | bytes 294944 | tf_op jit(solution)/shard_map/all_to_all | solution.py:109
  387.9 1.9 gather_fusion.1
  389.8 0.3 fusion.46
  390.1 0.6 add_convert_fusion.1
  (172 shorter events, 4.4 us)
Async XLA Ops:
  6.5 233.5 %copy-start = (bf16[1,2048,256]{2,1,0:T(8,128)(2,1)S(1)}, bf16[1,2048,256]{2,1,0:T(8,128)(2,1)}, u32[]{:S(2)}) copy-start(bf16[1,2048,256]{2,1,0:T(8,128)(2,1)} %param.33) | copy-start | bytes 3145732
  10.9 44.1 %copy-start.3 = (bf16[192,128]{1,0:T(8,128)(2,1)S(1)}, bf16[192,128]{1,0:T(8,128)(2,1)}, u32[]{:S(2)}) copy-start(bf16[192,128]{1,0:T(8,128)(2,1)} %param.22) | copy-start | bytes 147460
  12.6 41.7 %copy-start.4 = (f32[3,64,1,128]{3,1,2,0:T(8,128)}, f32[3,64,1,128]{3,1,2,0:T(8,128)S(1)}, u32[]{:S(2)}) copy-start(f32[3,64,1,128]{3,1,2,0:T(8,128)S(1)} %get-tuple-element.81) | copy-start | bytes 294916
  14.5 40.9 %copy-start.7 = (bf16[2,129,128]{2,1,0:T(8,128)(2,1)}, bf16[2,129,128]{2,1,0:T(8,128)(2,1)S(1)}, u32[]{:S(2)}) copy-start(bf16[2,129,128]{2,1,0:T(8,128)(2,1)S(1)} %all-gather.5) | copy-start | bytes 198148
  14.5 40.9 %copy-start.19 = (f32[128]{0:T(128)}, f32[128]{0:T(128)S(1)}, u32[]{:S(2)}) copy-start(f32[128]{0:T(128)S(1)} %fusion.382) | copy-start | bytes 1540
  15.1 40.3 %copy-start.16 = (f32[128]{0:T(128)}, f32[128]{0:T(128)S(1)}, u32[]{:S(2)}) copy-start(f32[128]{0:T(128)S(1)} %get-tuple-element.212) | copy-start | bytes 1540
  58.3 2.6 copy-start.6
  58.3 33.5 %copy-start.12 = (f32[3,128]{1,0:T(4,128)S(1)}, f32[3,128]{1,0:T(4,128)}, u32[]{:S(2)}) copy-start(f32[3,128]{1,0:T(4,128)} %get-tuple-element.225) | copy-start | bytes 4612
  60.2 31.1 %copy-start.8 = (bf16[2,129,128]{2,1,0:T(8,128)(2,1)}, bf16[2,129,128]{2,1,0:T(8,128)(2,1)S(1)}, u32[]{:S(2)}) copy-start(bf16[2,129,128]{2,1,0:T(8,128)(2,1)S(1)} %all-gather.7) | copy-start | bytes 198148
  92.1 3.2 copy-start.11
  93.3 2.4 copy-start.5
  93.3 2.6 copy-start.10
  93.3 2.6 copy-start.17
  93.3 2.6 copy-start.20
  93.3 2.6 copy-start.21
  93.3 2.6 copy-start.22
  93.3 2.6 copy-start.23
  93.4 2.6 copy-start.24
  93.4 2.6 copy-start.25
  93.4 2.6 copy-start.26
  93.4 2.6 copy-start.27
  93.4 2.6 copy-start.28
  93.4 2.6 copy-start.29
  93.4 2.6 copy-start.30
  93.4 2.6 copy-start.31
  93.4 2.6 copy-start.32
  93.4 2.6 copy-start.33
  93.5 2.6 copy-start.34
  93.5 2.6 copy-start.35
  93.5 2.6 copy-start.36
  93.5 2.6 copy-start.39
  95.3 2.3 copy-start.2
  95.3 2.3 copy-start.9
  95.3 2.3 copy-start.18
  98.1 8.7 %copy-start.13 = (s32[192,4]{0,1:T(4,128)S(1)}, s32[192,4]{0,1:T(4,128)}, u32[]{:S(2)}) copy-start(s32[192,4]{0,1:T(4,128)} %param.31) | copy-start | bytes 9220
  99.3 19.4 %all-to-all-start = ((bf16[16,12,2048]{2,1,0:T(8,128)(2,1)}), bf16[16,12,2048]{2,1,0:T(8,128)(2,1)S(1)}, u32[]{:S(2)}, u32[]{:S(2)}) async-start(bf16[16,12,2048]{2,1,0:T(8,128)(2,1)} %reshape.1657), calls=%async_computation | async-start | bytes 2097152 | tf_op jit(solution)/shard_map/all_to_all | solution.py:72
  120.0 17.0 %all-to-all-start.1 = ((bf16[16,12,2048]{2,1,0:T(8,128)(2,1)}), bf16[16,12,2048]{2,1,0:T(8,128)(2,1)S(1)}, u32[]{:S(2)}, u32[]{:S(2)}) async-start(bf16[16,12,2048]{2,1,0:T(8,128)(2,1)} %broadcast_in_dim.35), calls=%async_computation.1 | async-start | bytes 2097152 | tf_op jit(solution)/shard_map/all_to_all | solution.py:91
  124.9 115.1 %all-gather.12.cloned.1.call-start = ((), (), s32[]{:S(2)}) async-start(), calls=%async_computation.5 | async-start | bytes 5013504 | tf_op jit(solution)/shard_map/all_gather | solution.py:250
  125.2 13.1 %copy-start.1 = (bf16[192,2048]{1,0:T(8,128)(2,1)S(1)}, bf16[192,2048]{1,0:T(8,128)(2,1)}, u32[]{:S(2)}) copy-start(bf16[192,2048]{1,0:T(8,128)(2,1)} %param.20) | copy-start | bytes 2359300
  138.3 1.7 copy-start.14
  177.3 166.7 %all-gather.14.cloned.1.call-start = ((), (), s32[]{:S(2)}) async-start(), calls=%async_computation.6 | async-start | bytes 10027008 | tf_op jit(solution)/shard_map/all_gather | solution.py:260
  240.1 3.9 copy-start.37
  240.1 4.1 %copy-start.38 = (bf16[1,2048,256]{2,1,0:T(8,128)(2,1)S(1)}, bf16[1,2048,256]{2,1,0:T(8,128)(2,1)}, u32[]{:S(2)}) copy-start(bf16[1,2048,256]{2,1,0:T(8,128)(2,1)} %param.34) | copy-start | bytes 3145732
  350.5 17.4 %copy-start.15 = (f32[192,4]{0,1:T(4,128)S(1)}, f32[192,4]{0,1:T(4,128)}, u32[]{:S(2)}) copy-start(f32[192,4]{0,1:T(4,128)} %param.32) | copy-start | bytes 9220
  355.6 32.2 %all-to-all-start.4 = ((bf16[16,2,1,36,128]{4,1,3,2,0:T(2,128)(2,1)}), bf16[16,2,1,36,128]{4,1,3,2,0:T(2,128)(2,1)S(1)}, u32[]{:S(2)}, u32[]{:S(2)}) async-start(bf16[16,2,1,36,128]{4,1,3,2,0:T(2,128)(2,1)} %copy.64), calls=%async_computation.4 | async-start | bytes 589824 | tf_op jit(solution)/shard_map/all_to_all | solution.py:109
Sparse Core Ops, SparseCore 0:
  177.4 62.6 all-gather.11
  246.7 97.2 all-gather.13
where the time goes:
time: 398 us
  waiting for transfers between devices  197 us (49%)
  blocking collectives  108 us (27%)
  starting transfers between devices  25 us (6%)
  matrix products  21.1 us (5%)
  local copies, waits for them, and re-layouts  18.4 us (5%)
  between operations  14.5 us (4%)
  other arithmetic  12.4 us (3%)
    all_gather x1, waiting for transfers between devices, shards(): lax.all_gather(active, 'tp', axis=2, tiled=True)  97.4 us
    all_gather x4, blocking collectives, all_in_one(): both, at, found = (lax.all_gather(jnp.concatenate(lines), axis), 0, {})  71.3 us
    all_gather x1, waiting for transfers between devices, shards(): piece = lax.all_gather(arrived, 'tp', axis=2, tiled=True)  62.6 us
    all_to_all x1, blocking collectives, shards(): lax.all_to_all(buffer, SP, split_axis=0, concat_axis=1, tiled=True)  33.2 us
    all_to_all x1, waiting for transfers between devices, turned_blocks(): filled = lax.all_to_all(filled, axes[k], k, k, tiled=True)  19.8 us
    all_to_all x1, starting transfers between devices, turned_blocks(): filled = lax.all_to_all(filled, axes[k], k, k, tiled=True)  12.3 us
    all_to_all x1, waiting for transfers between devices, sent_and_summed(): pieces = lax.all_to_all(in_blocks(x, dim, length), axis, 0, 0, tiled=True)  9.91 us
  transfers between devices with their start and end apart: 5, of which 5 were waited for; matrix products, arithmetic and copies ran while one was open for 2% of the time, Pallas kernels for 0%

commit v1 on v0

--- a/solution.py
+++ b/solution.py
@@ -12,6 +12,19 @@
 eps_norm = 1e-06
 limit_value = 7.0
 alpha_value = 1.702
+
+
+def ring_gather(array, axis, dim):
+    ways = lax.axis_size(axis)
+    up = [(d, (d + 1) % ways) for d in range(ways)]
+    down = [(d, (d - 1) % ways) for d in range(ways)]
+    earlier, later = ([array], [array])
+    for _ in range(ways // 2):
+        earlier.append(lax.ppermute(earlier[-1], axis, up))
+    for _ in range((ways - 1) // 2):
+        later.append(lax.ppermute(later[-1], axis, down))
+    line = jnp.concatenate([*earlier[::-1], *later[1:]], axis=dim)
+    return jnp.roll(line, (lax.axis_index(axis) - ways // 2) * array.shape[dim], axis=dim)
 
 
 def filled_with(x, identity):
@@ -256,10 +269,7 @@
         jnp.bfloat16
     )
     produced = jnp.einsum(
-        "esf,efd->esd",
-        lax.all_gather(active, "tp", axis=2, tiled=True),
-        w_down,
-        preferred_element_type=jnp.float32,
+        "esf,efd->esd", ring_gather(active, "tp", 2), w_down, preferred_element_type=jnp.float32
     ).astype(jnp.bfloat16)
     returned = core_and_chips(produced, ("sp_0", "sp_1"), (1, 0), 1, 0)
     picked = returned.reshape(EXPERTS * CAP, part_width)[slot_index].astype(jnp.float32)

time: 398 us -> 458 us (1.15)
  the two profiles are of different devices: /device:TPU:2 before, /device:TPU:32 now
where the time goes in v1:
time: 458 us; the launch traced here: 456 us
  waiting for transfers between devices  164 us (36%)
  blocking collectives  106 us (23%)
  starting transfers between devices  91.8 us (20%)
  local copies, waits for them, and re-layouts  42.1 us (9%)
  matrix products  21.7 us (5%)
  between operations  14.7 us (3%)
  other arithmetic  14.5 us (3%)
    all_gather x4, blocking collectives, all_in_one(): both, at, found = (lax.all_gather(jnp.concatenate(lines), axis), 0, {})  71.1 us
    all_gather x1, waiting for transfers between devices, shards(): piece = lax.all_gather(arrived, 'tp', axis=2, tiled=True)  63.8 us
    ppermute x8, waiting for transfers between devices, ring_gather(): earlier.append(lax.ppermute(earlier[-1], axis, up))  61.1 us
    ppermute x7, starting transfers between devices, ring_gather(): later.append(lax.ppermute(later[-1], axis, down))  52 us
    all_to_all x1, blocking collectives, shards(): lax.all_to_all(buffer, SP, split_axis=0, concat_axis=1, tiled=True)  31.4 us
    unnamed x103, local copies, waits for them, and re-layouts  23.5 us
    all_to_all x1, waiting for transfers between devices, turned_blocks(): filled = lax.all_to_all(filled, axes[k], k, k, tiled=True)  19 us
    ppermute x8, starting transfers between devices, ring_gather(): earlier.append(lax.ppermute(earlier[-1], axis, up))  16.4 us
  transfers between devices with their start and end apart: 19, of which 14 were waited for; matrix products, arithmetic and copies ran while one was open for 5% of the time, Pallas kernels for 0%

profile of v1, /device:TPU:32, one launch (start us, length us, event | category | flops | bytes accessed | tf_op | source)
XLA Modules:
  0.0 455.5 jit_solution(5578979661529291351)
XLA Ops:
  10.4 1.7 while.26
  12.1 1.9 all-gather.4
  14.7 36.5 %all-gather.5 = bf16[16,129,128]{2,1,0:T(8,128)(2,1)S(1)} all-gather(bf16[1,129,128]{2,1,0:T(8,128)(2,1)S(1)} %maximum_bitcast_fusion.1), channel_id=3, replica_groups=mesh['sp_0'=16,'sp_1'=2,'tp'=16] {'sp_0'}, dimensions={0}, use_global_device_ids=true | all-gather | bytes 561408 | tf_op jit(solution)/shard_map/all_gather | solution.py:44
  54.4 1.7 while.27
  56.2 1.9 all-gather.6
  59.0 30.9 %all-gather.7 = bf16[16,129,128]{2,1,0:T(8,128)(2,1)S(1)} all-gather(bf16[1,129,128]{2,1,0:T(8,128)(2,1)S(1)} %maximum_bitcast_fusion.3), channel_id=5, replica_groups=mesh['sp_0'=16,'sp_1'=2,'tp'=16] {'sp_0'}, dimensions={0}, use_global_device_ids=true | all-gather | bytes 561408 | tf_op jit(solution)/shard_map/all_gather | solution.py:44
  94.9 1.5 fusion.48
  98.8 2.0 multiply_reduce_fusion.1
  100.8 1.5 convolution_convert_fusion
  102.3 1.2 reshape.1657
  103.5 7.0 %all-to-all-start = ((bf16[16,12,2048]{2,1,0:T(8,128)(2,1)}), bf16[16,12,2048]{2,1,0:T(8,128)(2,1)S(1)}, u32[]{:S(2)}, u32[]{:S(2)}) async-start(bf16[16,12,2048]{2,1,0:T(8,128)(2,1)} %reshape.1657), calls=%async_computation | async-start | bytes 2097152 | tf_op jit(solution)/shard_map/all_to_all | solution.py:85
  111.5 1.7 reduce-window.26
  113.9 10.0 %all-to-all-done = bf16[16,12,2048]{2,1,0:T(8,128)(2,1)S(1)} async-done(((bf16[16,12,2048]{2,1,0:T(8,128)(2,1)}), bf16[16,12,2048]{2,1,0:T(8,128)(2,1)S(1)}, u32[]{:S(2)}, u32[]{:S(2)}) %all-to-all-start) | async-done | bytes 786464 | tf_op jit(solution)/shard_map/all_to_all | solution.py:85
  125.2 3.7 all-to-all-start.1
  129.7 3.4 scatter_custom_fusion
  133.1 9.1 %all-to-all-done.1 = bf16[16,12,2048]{2,1,0:T(8,128)(2,1)S(1)} async-done(((bf16[16,12,2048]{2,1,0:T(8,128)(2,1)}), bf16[16,12,2048]{2,1,0:T(8,128)(2,1)S(1)}, u32[]{:S(2)}, u32[]{:S(2)}) %all-to-all-start.1) | async-done | bytes 786464 | tf_op jit(solution)/shard_map/all_to_all | solution.py:104
  142.1 1.3 reshape.1699
  143.5 1.7 multiply_reduce_fusion
  145.4 2.9 gather_fusion
  148.4 31.4 %all_to_all.32 = bf16[32,36,128]{2,1,0:T(8,128)(2,1)S(1)} all-to-all(bf16[32,36,128]{2,1,0:T(8,128)(2,1)S(1)} %reshape.1659), channel_id=1, replica_groups=mesh['sp_0'=16,'sp_1'=2,'tp'=16] {'sp_0','sp_1'}, dimensions={0} | all-to-all | bytes 589824 | tf_op jit(solution)/shard_map/all_to_all | solution.py:262
  180.6 63.8 %all-gather.10.cloned.1.call-done = bf16[1,1152,2048]{2,1,0:T(8,128)(2,1)} async-done(((bf16[1,1152,128]{2,1,0:T(8,128)(2,1)}), bf16[1,1152,2048]{2,1,0:T(8,128)(2,1)}) %all-gather.10.cloned.1.call-update) | async-done | bytes 4718608 | tf_op jit(solution)/shard_map/all_gather | solution.py:263
  244.4 3.9 fusion.28
  248.3 4.4 fusion.40
  252.7 3.1 collective-permute-start
  255.8 15.8 %collective-permute-done = bf16[1,1152,256]{1,2,0:T(8,128)(2,1)S(1)} collective-permute-done((bf16[1,1152,256]{1,2,0:T(8,128)(2,1)S(1)}, bf16[1,1152,256]{1,2,0:T(8,128)(2,1)S(1)}, u32[]{:S(2)}, u32[]{:S(2)}) %collective-permute-start) | collective-permute-done | bytes 589856 | tf_op jit(solution)/shard_map/ppermute | solution.py:23
  271.6 1.9 collective-permute-start.1
  273.6 7.2 %collective-permute-start.8 = (bf16[1,1152,256]{1,2,0:T(8,128)(2,1)S(1)}, bf16[1,1152,256]{1,2,0:T(8,128)(2,1)S(1)}, u32[]{:S(2)}, u32[]{:S(2)}) collective-permute-start(bf16[1,1152,256]{1,2,0:T(8,128)(2,1)S(1)} %fusion.40), channel_id=1, source_target_pairs={{0,15},{1,0},{2,1},{3,2},{4,3},{5,4},{6,5},{7,6},{8,7},{9,8},{10,9... | collective-permute-start | bytes 1769480 | tf_op jit(solution)/shard_map/ppermute | solution.py:25
  280.8 8.9 %collective-permute-done.1 = bf16[1,1152,256]{1,2,0:T(8,128)(2,1)S(1)} collective-permute-done((bf16[1,1152,256]{1,2,0:T(8,128)(2,1)S(1)}, bf16[1,1152,256]{1,2,0:T(8,128)(2,1)S(1)}, u32[]{:S(2)}, u32[]{:S(2)}) %collective-permute-start.1) | collective-permute-done | bytes 589856 | tf_op jit(solution)/shard_map/ppermute | solution.py:23
  289.7 1.9 collective-permute-start.2
  291.6 7.2 %collective-permute-start.9 = (bf16[1,1152,256]{1,2,0:T(8,128)(2,1)S(1)}, bf16[1,1152,256]{1,2,0:T(8,128)(2,1)S(1)}, u32[]{:S(2)}, u32[]{:S(2)}) collective-permute-start(bf16[1,1152,256]{1,2,0:T(8,128)(2,1)S(1)} %collective-permute-done.8), channel_id=1, source_target_pairs={{0,15},{1,0},{2,1},{3,2},{4,3},{5,4},{6,5},{7,6},{8,7},{9,8},{10,9... | collective-permute-start | bytes 1769480 | tf_op jit(solution)/shard_map/ppermute | solution.py:25
  298.9 8.0 %collective-permute-done.2 = bf16[1,1152,256]{1,2,0:T(8,128)(2,1)S(1)} collective-permute-done((bf16[1,1152,256]{1,2,0:T(8,128)(2,1)S(1)}, bf16[1,1152,256]{1,2,0:T(8,128)(2,1)S(1)}, u32[]{:S(2)}, u32[]{:S(2)}) %collective-permute-start.2) | collective-permute-done | bytes 589856 | tf_op jit(solution)/shard_map/ppermute | solution.py:23
  306.9 1.9 collective-permute-start.3
  308.8 7.2 %collective-permute-start.10 = (bf16[1,1152,256]{1,2,0:T(8,128)(2,1)S(1)}, bf16[1,1152,256]{1,2,0:T(8,128)(2,1)S(1)}, u32[]{:S(2)}, u32[]{:S(2)}) collective-permute-start(bf16[1,1152,256]{1,2,0:T(8,128)(2,1)S(1)} %collective-permute-done.9), channel_id=1, source_target_pairs={{0,15},{1,0},{2,1},{3,2},{4,3},{5,4},{6,5},{7,6},{8,7},{9,8},{10,9... | collective-permute-start | bytes 1769480 | tf_op jit(solution)/shard_map/ppermute | solution.py:25
  316.1 7.1 %collective-permute-done.3 = bf16[1,1152,256]{1,2,0:T(8,128)(2,1)S(1)} collective-permute-done((bf16[1,1152,256]{1,2,0:T(8,128)(2,1)S(1)}, bf16[1,1152,256]{1,2,0:T(8,128)(2,1)S(1)}, u32[]{:S(2)}, u32[]{:S(2)}) %collective-permute-start.3) | collective-permute-done | bytes 589856 | tf_op jit(solution)/shard_map/ppermute | solution.py:23
  323.2 1.9 collective-permute-start.4
  325.2 7.2 %collective-permute-start.11 = (bf16[1,1152,256]{1,2,0:T(8,128)(2,1)S(1)}, bf16[1,1152,256]{1,2,0:T(8,128)(2,1)S(1)}, u32[]{:S(2)}, u32[]{:S(2)}) collective-permute-start(bf16[1,1152,256]{1,2,0:T(8,128)(2,1)S(1)} %collective-permute-done.10), channel_id=1, source_target_pairs={{0,15},{1,0},{2,1},{3,2},{4,3},{5,4},{6,5},{7,6},{8,7},{9,8},{10,9... | collective-permute-start | bytes 1769480 | tf_op jit(solution)/shard_map/ppermute | solution.py:25
  332.4 6.3 %collective-permute-done.4 = bf16[1,1152,256]{1,2,0:T(8,128)(2,1)S(1)} collective-permute-done((bf16[1,1152,256]{1,2,0:T(8,128)(2,1)S(1)}, bf16[1,1152,256]{1,2,0:T(8,128)(2,1)S(1)}, u32[]{:S(2)}, u32[]{:S(2)}) %collective-permute-start.4) | collective-permute-done | bytes 589856 | tf_op jit(solution)/shard_map/ppermute | solution.py:23
  338.7 1.9 collective-permute-start.5
  341.5 7.2 %collective-permute-start.12 = (bf16[1,1152,256]{1,2,0:T(8,128)(2,1)S(1)}, bf16[1,1152,256]{1,2,0:T(8,128)(2,1)}, u32[]{:S(2)}, u32[]{:S(2)}) collective-permute-start(bf16[1,1152,256]{1,2,0:T(8,128)(2,1)S(1)} %collective-permute-done.11), channel_id=1, source_target_pairs={{0,15},{1,0},{2,1},{3,2},{4,3},{5,4},{6,5},{7,6},{8,7},{9,8},{10,9... | collective-permute-start | bytes 1769480 | tf_op jit(solution)/shard_map/ppermute | solution.py:25
  348.7 5.1 %collective-permute-done.5 = bf16[1,1152,256]{1,2,0:T(8,128)(2,1)S(1)} collective-permute-done((bf16[1,1152,256]{1,2,0:T(8,128)(2,1)S(1)}, bf16[1,1152,256]{1,2,0:T(8,128)(2,1)S(1)}, u32[]{:S(2)}, u32[]{:S(2)}) %collective-permute-start.5) | collective-permute-done | bytes 589856 | tf_op jit(solution)/shard_map/ppermute | solution.py:23
  353.8 1.9 collective-permute-start.6
  356.1 7.8 %collective-permute-start.13 = (bf16[1,1152,256]{1,2,0:T(8,128)(2,1)}, bf16[1,1152,256]{1,2,0:T(8,128)(2,1)}, u32[]{:S(2)}, u32[]{:S(2)}) collective-permute-start(bf16[1,1152,256]{1,2,0:T(8,128)(2,1)} %collective-permute-done.12), channel_id=1, source_target_pairs={{0,15},{1,0},{2,1},{3,2},{4,3},{5,4},{6,5},{7,6},{8,7},{9,8},{10,9... | collective-permute-start | bytes 1769480 | tf_op jit(solution)/shard_map/ppermute | solution.py:25
  363.9 5.1 %collective-permute-done.6 = bf16[1,1152,256]{1,2,0:T(8,128)(2,1)} collective-permute-done((bf16[1,1152,256]{1,2,0:T(8,128)(2,1)S(1)}, bf16[1,1152,256]{1,2,0:T(8,128)(2,1)}, u32[]{:S(2)}, u32[]{:S(2)}) %collective-permute-start.6) | collective-permute-done | bytes 589856 | tf_op jit(solution)/shard_map/ppermute | solution.py:23
  369.0 1.9 collective-permute-start.7
  371.6 8.0 %collective-permute-start.14 = (bf16[1,1152,256]{1,2,0:T(8,128)(2,1)}, bf16[1,1152,256]{1,2,0:T(8,128)(2,1)S(1)}, u32[]{:S(2)}, u32[]{:S(2)}) collective-permute-start(bf16[1,1152,256]{1,2,0:T(8,128)(2,1)} %collective-permute-done.13), channel_id=1, source_target_pairs={{0,15},{1,0},{2,1},{3,2},{4,3},{5,4},{6,5},{7,6},{8,7},{9,8},{10,9... | collective-permute-start | bytes 1769480 | tf_op jit(solution)/shard_map/ppermute | solution.py:25
  379.6 4.8 %collective-permute-done.7 = bf16[1,1152,256]{1,2,0:T(8,128)(2,1)} collective-permute-done((bf16[1,1152,256]{1,2,0:T(8,128)(2,1)}, bf16[1,1152,256]{1,2,0:T(8,128)(2,1)}, u32[]{:S(2)}, u32[]{:S(2)}) %collective-permute-start.7) | collective-permute-done | bytes 589856 | tf_op jit(solution)/shard_map/ppermute | solution.py:23
  385.5 1.1 constant_dynamic-update-slice_fusion.30
  386.7 1.1 constant_dynamic-update-slice_fusion.29
  387.8 1.1 constant_dynamic-update-slice_fusion.28
  388.9 1.1 constant_dynamic-update-slice_fusion.27
  390.1 1.1 constant_dynamic-update-slice_fusion.26
  391.2 1.1 constant_dynamic-update-slice_fusion.25
  392.3 1.1 constant_dynamic-update-slice_fusion.24
  393.6 1.1 constant_dynamic-update-slice_fusion.22
  394.7 1.1 constant_dynamic-update-slice_fusion.21
  395.8 1.1 constant_dynamic-update-slice_fusion.20
  397.0 1.1 constant_dynamic-update-slice_fusion.19
  398.1 1.1 constant_dynamic-update-slice_fusion.18
  399.3 1.1 constant_dynamic-update-slice_fusion.17
  406.1 2.7 fusion.43
  408.9 4.0 all_to_all.33
  413.9 12.7 %all-to-all-start.4 = ((bf16[16,2,1,36,128]{4,1,3,2,0:T(2,128)(2,1)}), bf16[16,2,1,36,128]{4,1,3,2,0:T(2,128)(2,1)S(1)}, u32[]{:S(2)}, u32[]{:S(2)}) async-start(bf16[16,2,1,36,128]{4,1,3,2,0:T(2,128)(2,1)} %copy.64), calls=%async_computation.4 | async-start | bytes 589824 | tf_op jit(solution)/shard_map/all_to_all | solution.py:122
  426.7 19.0 %all-to-all-done.4 = bf16[16,2,1,36,128]{4,1,3,2,0:T(2,128)(2,1)S(1)} async-done(((bf16[16,2,1,36,128]{4,1,3,2,0:T(2,128)(2,1)}), bf16[16,2,1,36,128]{4,1,3,2,0:T(2,128)(2,1)S(1)}, u32[]{:S(2)}, u32[]{:S(2)}) %all-to-all-start.4) | async-done | bytes 294944 | tf_op jit(solution)/shard_map/all_to_all | solution.py:122
  445.8 1.9 gather_fusion.1
  (219 shorter events, 34.4 us)
Async XLA Ops:
  6.5 237.9 %copy-start = (bf16[1,2048,256]{2,1,0:T(8,128)(2,1)S(1)}, bf16[1,2048,256]{2,1,0:T(8,128)(2,1)}, u32[]{:S(2)}) copy-start(bf16[1,2048,256]{2,1,0:T(8,128)(2,1)} %param.33) | copy-start | bytes 3145732
  6.5 136.9 %copy-start.21 = (bf16[192,2048]{1,0:T(8,128)(2,1)S(1)}, bf16[192,2048]{1,0:T(8,128)(2,1)}, u32[]{:S(2)}) copy-start(bf16[192,2048]{1,0:T(8,128)(2,1)} %param.20) | copy-start | bytes 2359300
  12.1 39.8 %copy-start.23 = (f32[3,64,1,128]{3,1,2,0:T(8,128)}, f32[3,64,1,128]{3,1,2,0:T(8,128)S(1)}, u32[]{:S(2)}) copy-start(f32[3,64,1,128]{3,1,2,0:T(8,128)S(1)} %get-tuple-element.81) | copy-start | bytes 294916
  14.0 39.8 %copy-start.25 = (bf16[2,129,128]{2,1,0:T(8,128)(2,1)}, bf16[2,129,128]{2,1,0:T(8,128)(2,1)S(1)}, u32[]{:S(2)}) copy-start(bf16[2,129,128]{2,1,0:T(8,128)(2,1)S(1)} %all-gather.4) | copy-start | bytes 198148
  14.0 39.8 %copy-start.31 = (f32[128]{0:T(128)}, f32[128]{0:T(128)S(1)}, u32[]{:S(2)}) copy-start(f32[128]{0:T(128)S(1)} %fusion.392) | copy-start | bytes 1540
  14.5 39.2 %copy-start.29 = (f32[128]{0:T(128)}, f32[128]{0:T(128)S(1)}, u32[]{:S(2)}) copy-start(f32[128]{0:T(128)S(1)} %get-tuple-element.212) | copy-start | bytes 1540
  51.1 3.0 copy-start.22
  56.1 2.5 copy-start.24
  58.0 0.6 copy-start.26
  58.0 0.6 copy-start.32
  58.5 0.5 copy-start.30
  93.5 51.7 %copy-start.27 = (f32[2048]{0:T(1024)S(1)}, f32[2048]{0:T(1024)}, u32[]{:S(2)}) copy-start(f32[2048]{0:T(1024)} %param.30) | copy-start | bytes 24580
  103.5 20.4 %all-to-all-start = ((bf16[16,12,2048]{2,1,0:T(8,128)(2,1)}), bf16[16,12,2048]{2,1,0:T(8,128)(2,1)S(1)}, u32[]{:S(2)}, u32[]{:S(2)}) async-start(bf16[16,12,2048]{2,1,0:T(8,128)(2,1)} %reshape.1657), calls=%async_computation | async-start | bytes 2097152 | tf_op jit(solution)/shard_map/all_to_all | solution.py:85
  125.2 17.0 %all-to-all-start.1 = ((bf16[16,12,2048]{2,1,0:T(8,128)(2,1)}), bf16[16,12,2048]{2,1,0:T(8,128)(2,1)S(1)}, u32[]{:S(2)}, u32[]{:S(2)}) async-start(bf16[16,12,2048]{2,1,0:T(8,128)(2,1)} %broadcast_in_dim.35), calls=%async_computation.1 | async-start | bytes 2097152 | tf_op jit(solution)/shard_map/all_to_all | solution.py:104
  128.8 115.6 %all-gather.10.cloned.1.call-start = ((), (), s32[]{:S(2)}) async-start(), calls=%async_computation.5 | async-start | bytes 5013504 | tf_op jit(solution)/shard_map/all_gather | solution.py:263
  252.7 18.9 %collective-permute-start = (bf16[1,1152,256]{1,2,0:T(8,128)(2,1)S(1)}, bf16[1,1152,256]{1,2,0:T(8,128)(2,1)S(1)}, u32[]{:S(2)}, u32[]{:S(2)}) collective-permute-start(bf16[1,1152,256]{1,2,0:T(8,128)(2,1)S(1)} %fusion.40), channel_id=1, source_target_pairs={{0,1},{1,2},{2,3},{3,4},{4,5},{5,6},{6,7},{7,8},{8,9},{9,10},{10,1... | collective-permute-start | bytes 1769480 | tf_op jit(solution)/shard_map/ppermute | solution.py:23
  271.6 20.0 %copy-start.1 = (bf16[1,1152,256]{1,2,0:T(8,128)(2,1)}, bf16[1,1152,256]{1,2,0:T(8,128)(2,1)S(1)}, u32[]{:S(2)}) copy-start(bf16[1,1152,256]{1,2,0:T(8,128)(2,1)S(1)} %collective-permute-done) | copy-start | bytes 1769476
  271.6 18.0 %collective-permute-start.1 = (bf16[1,1152,256]{1,2,0:T(8,128)(2,1)S(1)}, bf16[1,1152,256]{1,2,0:T(8,128)(2,1)S(1)}, u32[]{:S(2)}, u32[]{:S(2)}) collective-permute-start(bf16[1,1152,256]{1,2,0:T(8,128)(2,1)S(1)} %collective-permute-done), channel_id=1, source_target_pairs={{0,1},{1,2},{2,3},{3,4},{4,5},{5,6},{6,7},{7,8},{8,9},{9,10},{10,1... | collective-permute-start | bytes 1769480 | tf_op jit(solution)/shard_map/ppermute | solution.py:23
  273.6 18.1 %collective-permute-start.8 = (bf16[1,1152,256]{1,2,0:T(8,128)(2,1)S(1)}, bf16[1,1152,256]{1,2,0:T(8,128)(2,1)S(1)}, u32[]{:S(2)}, u32[]{:S(2)}) collective-permute-start(bf16[1,1152,256]{1,2,0:T(8,128)(2,1)S(1)} %fusion.40), channel_id=1, source_target_pairs={{0,15},{1,0},{2,1},{3,2},{4,3},{5,4},{6,5},{7,6},{8,7},{9,8},{10,9... | collective-permute-start | bytes 1769480 | tf_op jit(solution)/shard_map/ppermute | solution.py:25
  289.7 19.1 %copy-start.5 = (bf16[1,1152,256]{1,2,0:T(8,128)(2,1)}, bf16[1,1152,256]{1,2,0:T(8,128)(2,1)S(1)}, u32[]{:S(2)}) copy-start(bf16[1,1152,256]{1,2,0:T(8,128)(2,1)S(1)} %collective-permute-done.1) | copy-start | bytes 1769476
  289.7 17.2 %collective-permute-start.2 = (bf16[1,1152,256]{1,2,0:T(8,128)(2,1)S(1)}, bf16[1,1152,256]{1,2,0:T(8,128)(2,1)S(1)}, u32[]{:S(2)}, u32[]{:S(2)}) collective-permute-start(bf16[1,1152,256]{1,2,0:T(8,128)(2,1)S(1)} %collective-permute-done.1), channel_id=1, source_target_pairs={{0,1},{1,2},{2,3},{3,4},{4,5},{5,6},{6,7},{7,8},{8,9},{9,10},{10,1... | collective-permute-start | bytes 1769480 | tf_op jit(solution)/shard_map/ppermute | solution.py:23
  291.6 7.3 %copy-start.3 = (bf16[1,1152,256]{1,2,0:T(8,128)(2,1)}, bf16[1,1152,256]{1,2,0:T(8,128)(2,1)S(1)}, u32[]{:S(2)}) copy-start(bf16[1,1152,256]{1,2,0:T(8,128)(2,1)S(1)} %collective-permute-done.8) | copy-start | bytes 1769476
  291.6 17.2 %collective-permute-start.9 = (bf16[1,1152,256]{1,2,0:T(8,128)(2,1)S(1)}, bf16[1,1152,256]{1,2,0:T(8,128)(2,1)S(1)}, u32[]{:S(2)}, u32[]{:S(2)}) collective-permute-start(bf16[1,1152,256]{1,2,0:T(8,128)(2,1)S(1)} %collective-permute-done.8), channel_id=1, source_target_pairs={{0,15},{1,0},{2,1},{3,2},{4,3},{5,4},{6,5},{7,6},{8,7},{9,8},{10,9... | collective-permute-start | bytes 1769480 | tf_op jit(solution)/shard_map/ppermute | solution.py:25
  306.9 18.3 %copy-start.9 = (bf16[1,1152,256]{1,2,0:T(8,128)(2,1)}, bf16[1,1152,256]{1,2,0:T(8,128)(2,1)S(1)}, u32[]{:S(2)}) copy-start(bf16[1,1152,256]{1,2,0:T(8,128)(2,1)S(1)} %collective-permute-done.2) | copy-start | bytes 1769476
  306.9 16.3 %collective-permute-start.3 = (bf16[1,1152,256]{1,2,0:T(8,128)(2,1)S(1)}, bf16[1,1152,256]{1,2,0:T(8,128)(2,1)S(1)}, u32[]{:S(2)}, u32[]{:S(2)}) collective-permute-start(bf16[1,1152,256]{1,2,0:T(8,128)(2,1)S(1)} %collective-permute-done.2), channel_id=1, source_target_pairs={{0,1},{1,2},{2,3},{3,4},{4,5},{5,6},{6,7},{7,8},{8,9},{9,10},{10,1... | collective-permute-start | bytes 1769480 | tf_op jit(solution)/shard_map/ppermute | solution.py:23
  308.8 7.3 %copy-start.7 = (bf16[1,1152,256]{1,2,0:T(8,128)(2,1)}, bf16[1,1152,256]{1,2,0:T(8,128)(2,1)S(1)}, u32[]{:S(2)}) copy-start(bf16[1,1152,256]{1,2,0:T(8,128)(2,1)S(1)} %collective-permute-done.9) | copy-start | bytes 1769476
  308.8 16.3 %collective-permute-start.10 = (bf16[1,1152,256]{1,2,0:T(8,128)(2,1)S(1)}, bf16[1,1152,256]{1,2,0:T(8,128)(2,1)S(1)}, u32[]{:S(2)}, u32[]{:S(2)}) collective-permute-start(bf16[1,1152,256]{1,2,0:T(8,128)(2,1)S(1)} %collective-permute-done.9), channel_id=1, source_target_pairs={{0,15},{1,0},{2,1},{3,2},{4,3},{5,4},{6,5},{7,6},{8,7},{9,8},{10,9... | collective-permute-start | bytes 1769480 | tf_op jit(solution)/shard_map/ppermute | solution.py:25
  323.2 32.9 %copy-start.15 = (bf16[1,1152,256]{1,2,0:T(8,128)(2,1)}, bf16[1,1152,256]{1,2,0:T(8,128)(2,1)S(1)}, u32[]{:S(2)}) copy-start(bf16[1,1152,256]{1,2,0:T(8,128)(2,1)S(1)} %collective-permute-done.3) | copy-start | bytes 1769476
  323.2 15.5 %collective-permute-start.4 = (bf16[1,1152,256]{1,2,0:T(8,128)(2,1)S(1)}, bf16[1,1152,256]{1,2,0:T(8,128)(2,1)S(1)}, u32[]{:S(2)}, u32[]{:S(2)}) collective-permute-start(bf16[1,1152,256]{1,2,0:T(8,128)(2,1)S(1)} %collective-permute-done.3), channel_id=1, source_target_pairs={{0,1},{1,2},{2,3},{3,4},{4,5},{5,6},{6,7},{7,8},{8,9},{9,10},{10,1... | collective-permute-start | bytes 1769480 | tf_op jit(solution)/shard_map/ppermute | solution.py:23
  325.2 7.3 %copy-start.11 = (bf16[1,1152,256]{1,2,0:T(8,128)(2,1)}, bf16[1,1152,256]{1,2,0:T(8,128)(2,1)S(1)}, u32[]{:S(2)}) copy-start(bf16[1,1152,256]{1,2,0:T(8,128)(2,1)S(1)} %collective-permute-done.10) | copy-start | bytes 1769476
  325.2 15.5 %collective-permute-start.11 = (bf16[1,1152,256]{1,2,0:T(8,128)(2,1)S(1)}, bf16[1,1152,256]{1,2,0:T(8,128)(2,1)S(1)}, u32[]{:S(2)}, u32[]{:S(2)}) collective-permute-start(bf16[1,1152,256]{1,2,0:T(8,128)(2,1)S(1)} %collective-permute-done.10), channel_id=1, source_target_pairs={{0,15},{1,0},{2,1},{3,2},{4,3},{5,4},{6,5},{7,6},{8,7},{9,8},{10,9... | collective-permute-start | bytes 1769480 | tf_op jit(solution)/shard_map/ppermute | solution.py:25
  338.7 25.2 %copy-start.17 = (bf16[1,1152,256]{1,2,0:T(8,128)(2,1)}, bf16[1,1152,256]{1,2,0:T(8,128)(2,1)S(1)}, u32[]{:S(2)}) copy-start(bf16[1,1152,256]{1,2,0:T(8,128)(2,1)S(1)} %collective-permute-done.4) | copy-start | bytes 1769476
  338.7 15.1 %collective-permute-start.5 = (bf16[1,1152,256]{1,2,0:T(8,128)(2,1)S(1)}, bf16[1,1152,256]{1,2,0:T(8,128)(2,1)S(1)}, u32[]{:S(2)}, u32[]{:S(2)}) collective-permute-start(bf16[1,1152,256]{1,2,0:T(8,128)(2,1)S(1)} %collective-permute-done.4), channel_id=1, source_target_pairs={{0,1},{1,2},{2,3},{3,4},{4,5},{5,6},{6,7},{7,8},{8,9},{9,10},{10,1... | collective-permute-start | bytes 1769480 | tf_op jit(solution)/shard_map/ppermute | solution.py:23
  340.6 0.8 copy-start.13
  341.5 14.6 %collective-permute-start.12 = (bf16[1,1152,256]{1,2,0:T(8,128)(2,1)S(1)}, bf16[1,1152,256]{1,2,0:T(8,128)(2,1)}, u32[]{:S(2)}, u32[]{:S(2)}) collective-permute-start(bf16[1,1152,256]{1,2,0:T(8,128)(2,1)S(1)} %collective-permute-done.11), channel_id=1, source_target_pairs={{0,15},{1,0},{2,1},{3,2},{4,3},{5,4},{6,5},{7,6},{8,7},{9,8},{10,9... | collective-permute-start | bytes 1769480 | tf_op jit(solution)/shard_map/ppermute | solution.py:25
  353.8 15.2 %copy-start.19 = (bf16[1,1152,256]{1,2,0:T(8,128)(2,1)}, bf16[1,1152,256]{1,2,0:T(8,128)(2,1)S(1)}, u32[]{:S(2)}) copy-start(bf16[1,1152,256]{1,2,0:T(8,128)(2,1)S(1)} %collective-permute-done.5) | copy-start | bytes 1769476
  353.8 15.2 %collective-permute-start.6 = (bf16[1,1152,256]{1,2,0:T(8,128)(2,1)S(1)}, bf16[1,1152,256]{1,2,0:T(8,128)(2,1)}, u32[]{:S(2)}, u32[]{:S(2)}) collective-permute-start(bf16[1,1152,256]{1,2,0:T(8,128)(2,1)S(1)} %collective-permute-done.5), channel_id=1, source_target_pairs={{0,1},{1,2},{2,3},{3,4},{4,5},{5,6},{6,7},{7,8},{8,9},{9,10},{10,1... | collective-permute-start | bytes 1769480 | tf_op jit(solution)/shard_map/ppermute | solution.py:23
  356.1 15.5 %collective-permute-start.13 = (bf16[1,1152,256]{1,2,0:T(8,128)(2,1)}, bf16[1,1152,256]{1,2,0:T(8,128)(2,1)}, u32[]{:S(2)}, u32[]{:S(2)}) collective-permute-start(bf16[1,1152,256]{1,2,0:T(8,128)(2,1)} %collective-permute-done.12), channel_id=1, source_target_pairs={{0,15},{1,0},{2,1},{3,2},{4,3},{5,4},{6,5},{7,6},{8,7},{9,8},{10,9... | collective-permute-start | bytes 1769480 | tf_op jit(solution)/shard_map/ppermute | solution.py:25
  369.0 15.4 %collective-permute-start.7 = (bf16[1,1152,256]{1,2,0:T(8,128)(2,1)}, bf16[1,1152,256]{1,2,0:T(8,128)(2,1)}, u32[]{:S(2)}, u32[]{:S(2)}) collective-permute-start(bf16[1,1152,256]{1,2,0:T(8,128)(2,1)} %collective-permute-done.6), channel_id=1, source_target_pairs={{0,1},{1,2},{2,3},{3,4},{4,5},{5,6},{6,7},{7,8},{8,9},{9,10},{10,1... | collective-permute-start | bytes 1769480 | tf_op jit(solution)/shard_map/ppermute | solution.py:23
  370.9 31.8 %copy-start.20 = (bf16[1,1152,256]{1,2,0:T(8,128)(2,1)S(1)}, bf16[1,1152,256]{1,2,0:T(8,128)(2,1)}, u32[]{:S(2)}) copy-start(bf16[1,1152,256]{1,2,0:T(8,128)(2,1)} %copy-done.19) | copy-start | bytes 1769476
  371.0 31.9 %copy-start.18 = (bf16[1,1152,256]{1,2,0:T(8,128)(2,1)S(1)}, bf16[1,1152,256]{1,2,0:T(8,128)(2,1)}, u32[]{:S(2)}) copy-start(bf16[1,1152,256]{1,2,0:T(8,128)(2,1)} %copy-done.17) | copy-start | bytes 1769476
  371.0 32.0 %copy-start.16 = (bf16[1,1152,256]{1,2,0:T(8,128)(2,1)S(1)}, bf16[1,1152,256]{1,2,0:T(8,128)(2,1)}, u32[]{:S(2)}) copy-start(bf16[1,1152,256]{1,2,0:T(8,128)(2,1)} %copy-done.15) | copy-start | bytes 1769476
  371.0 32.0 %copy-start.10 = (bf16[1,1152,256]{1,2,0:T(8,128)(2,1)S(1)}, bf16[1,1152,256]{1,2,0:T(8,128)(2,1)}, u32[]{:S(2)}) copy-start(bf16[1,1152,256]{1,2,0:T(8,128)(2,1)} %copy-done.9) | copy-start | bytes 1769476
  371.0 32.1 %copy-start.6 = (bf16[1,1152,256]{1,2,0:T(8,128)(2,1)S(1)}, bf16[1,1152,256]{1,2,0:T(8,128)(2,1)}, u32[]{:S(2)}) copy-start(bf16[1,1152,256]{1,2,0:T(8,128)(2,1)} %copy-done.5) | copy-start | bytes 1769476
  371.0 32.2 %copy-start.2 = (bf16[1,1152,256]{1,2,0:T(8,128)(2,1)S(1)}, bf16[1,1152,256]{1,2,0:T(8,128)(2,1)}, u32[]{:S(2)}) copy-start(bf16[1,1152,256]{1,2,0:T(8,128)(2,1)} %copy-done.1) | copy-start | bytes 1769476
  371.0 32.4 %copy-start.4 = (bf16[1,1152,256]{1,2,0:T(8,128)(2,1)S(1)}, bf16[1,1152,256]{1,2,0:T(8,128)(2,1)}, u32[]{:S(2)}) copy-start(bf16[1,1152,256]{1,2,0:T(8,128)(2,1)} %copy-done.3) | copy-start | bytes 1769476
  371.0 32.4 %copy-start.8 = (bf16[1,1152,256]{1,2,0:T(8,128)(2,1)S(1)}, bf16[1,1152,256]{1,2,0:T(8,128)(2,1)}, u32[]{:S(2)}) copy-start(bf16[1,1152,256]{1,2,0:T(8,128)(2,1)} %copy-done.7) | copy-start | bytes 1769476
  371.0 32.5 %copy-start.12 = (bf16[1,1152,256]{1,2,0:T(8,128)(2,1)S(1)}, bf16[1,1152,256]{1,2,0:T(8,128)(2,1)}, u32[]{:S(2)}) copy-start(bf16[1,1152,256]{1,2,0:T(8,128)(2,1)} %copy-done.11) | copy-start | bytes 1769476
  371.0 32.6 %copy-start.14 = (bf16[1,1152,256]{1,2,0:T(8,128)(2,1)S(1)}, bf16[1,1152,256]{1,2,0:T(8,128)(2,1)}, u32[]{:S(2)}) copy-start(bf16[1,1152,256]{1,2,0:T(8,128)(2,1)} %copy-done.13) | copy-start | bytes 1769476
  371.0 35.0 %copy-start.33 = (bf16[1,4096,128]{2,1,0:T(8,128)(2,1)S(1)}, bf16[1,4096,128]{2,1,0:T(8,128)(2,1)}, u32[]{:S(2)}) copy-start(bf16[1,4096,128]{2,1,0:T(8,128)(2,1)} %param.35) | copy-start | bytes 3145732
  371.6 28.8 %collective-permute-start.14 = (bf16[1,1152,256]{1,2,0:T(8,128)(2,1)}, bf16[1,1152,256]{1,2,0:T(8,128)(2,1)S(1)}, u32[]{:S(2)}, u32[]{:S(2)}) collective-permute-start(bf16[1,1152,256]{1,2,0:T(8,128)(2,1)} %collective-permute-done.13), channel_id=1, source_target_pairs={{0,15},{1,0},{2,1},{3,2},{4,3},{5,4},{6,5},{7,6},{8,7},{9,8},{10,9... | collective-permute-start | bytes 1769480 | tf_op jit(solution)/shard_map/ppermute | solution.py:25
  398.1 28.5 %copy-start.28 = (f32[192,4]{0,1:T(4,128)S(1)}, f32[192,4]{0,1:T(4,128)}, u32[]{:S(2)}) copy-start(f32[192,4]{0,1:T(4,128)} %param.32) | copy-start | bytes 9220
  413.9 31.9 %all-to-all-start.4 = ((bf16[16,2,1,36,128]{4,1,3,2,0:T(2,128)(2,1)}), bf16[16,2,1,36,128]{4,1,3,2,0:T(2,128)(2,1)S(1)}, u32[]{:S(2)}, u32[]{:S(2)}) async-start(bf16[16,2,1,36,128]{4,1,3,2,0:T(2,128)(2,1)} %copy.64), calls=%async_computation.4 | async-start | bytes 589824 | tf_op jit(solution)/shard_map/all_to_all | solution.py:122
Sparse Core Ops, SparseCore 0:
  180.7 63.6 all-gather.9
